TPU v7x, 32 devices: a whole 2x2x4 slice. The times are simulated.
32 devices in a mesh: sp: 8 (over z, x), tp: 4 (over y, core).
Axes of the slice: x: 2, y: 2, z: 4, core: 2. Of those that a mesh axis runs over, the one named last changes fastest.
Arguments:
- tokens: bfloat16 [6144, 2048], P(('sp', 'tp')), may hold values from -6 to 6
- norm_gain: bfloat16 [2048], replicated, may hold values from 0.099609375 to 1.8984375
- conv_value_w: bfloat16 [2048, 2048], P('sp', 'tp'), may hold values from -0.125 to 0.125
- conv_gate_w: bfloat16 [2048, 2048], P('sp', 'tp'), may hold values from -0.125 to 0.125
- rnn_input_w: bfloat16 [2048, 2560], P('sp', 'tp'), may hold values from -0.125 to 0.125
- rnn_gate_w: bfloat16 [2048, 2560], P('sp', 'tp'), may hold values from -0.125 to 0.125
- conv_kernel: bfloat16 [31, 2048], P(None, 'tp'), may hold values from -3 to 3
- conv_norm_gain: bfloat16 [2048], P('tp'), may hold values from 0.099609375 to 1.8984375
- conv_norm_shift: bfloat16 [2048], P('tp'), may hold values from -3 to 3
- short_kernel: bfloat16 [4, 2560], P(None, 'tp'), may hold values from -3 to 3
- recur_map: bfloat16 [16, 160, 160], P('tp'), may hold values from -0.5 to 0.5
- input_map: bfloat16 [16, 160, 160], P('tp'), may hold values from -0.5 to 0.5
- decay_param: float32 [2560], P('tp'), may hold values from 4.5 to 16
- decay_shift: float32 [6144, 16], P('sp', 'tp'), may hold values from -1.1 to 0
- initial_state: float32 [2560], P('tp'), may hold values from -5 to 5
- conv_out_w: bfloat16 [2048, 2048], P('tp', 'sp'), may hold values from -0.125 to 0.125
- rnn_out_w: bfloat16 [2560, 2048], P('tp', 'sp'), may hold values from -0.125 to 0.125
Outputs:
- mixed: bfloat16 [6144, 2048], P(('sp', 'tp'))
All inputs are finite; a program needn't handle non-finite values.
Results may differ from a plain program's by a relative error of at most 0.015.
Values may be sent and summed in bfloat16 or wider, within the bound.
A program may use at most 128 MiB of HBM per device.

v0:
```python
import jax
import jax.numpy as jnp
from jax import lax
from jax.sharding import PartitionSpec as P

EPS = 1e-06
EXPONENT = 8.0


def shifted(x, axis, by):
    peers = lax.axis_size(axis)
    pairs = [(i, i + by) for i in range(peers) if 0 <= i + by < peers]
    return lax.ppermute(x, axis, pairs)


def entering_2(part, axis, combine, identity):
    place = lax.axis_index(axis)
    gathered = jax.tree.map(lambda a: lax.all_gather(a, axis), part)
    state = jax.tree.map(lambda a, e: jnp.zeros_like(a) + jnp.asarray(e, a.dtype), part, identity)

    def one(step, state):
        return combine(
            state, jax.tree.map(lambda a: lax.dynamic_index_in_dim(a, step, 0, False), gathered)
        )

    return lax.fori_loop(0, place, one, state)


def causal_taps(extended, kernel, length):
    result = jnp.zeros((length, extended.shape[1]), jnp.float32)
    for offset in range(kernel.shape[0]):
        result = result + kernel[offset].astype(jnp.float32) * extended[offset : offset + length]
    return result


def linear_pair(earlier, later):
    return (earlier[0] * later[0], later[0] * earlier[1] + later[1])


def block_diagonal(values, maps):
    row_count = values.shape[0]
    grouped = values.reshape(row_count, maps.shape[0], maps.shape[1])
    mapped = jnp.einsum("rhi,hij->rhj", grouped, maps, preferred_element_type=jnp.float32)
    return mapped.reshape(row_count, -1)


def local(
    tokens,
    norm_gain,
    conv_value_w,
    conv_gate_w,
    rnn_input_w,
    rnn_gate_w,
    conv_kernel,
    conv_norm_gain,
    conv_norm_shift,
    short_kernel,
    recur_map,
    input_map,
    decay_param,
    decay_shift,
    initial_state,
    conv_out_w,
    rnn_out_w,
):
    as_float = tokens.astype(jnp.float32)
    scale = lax.rsqrt(jnp.mean(as_float * as_float, axis=1, keepdims=True) + EPS)
    normed = (as_float * scale * norm_gain.astype(jnp.float32)).astype(jnp.bfloat16)
    edges = [0]
    for weight in (conv_value_w, conv_gate_w, rnn_input_w, rnn_gate_w):
        edges.append(edges[-1] + weight.shape[1])
    gathered = (
        lax.all_gather(conv_value_w, "sp", axis=0, tiled=True),
        lax.all_gather(conv_gate_w, "sp", axis=0, tiled=True),
        lax.all_gather(rnn_input_w, "sp", axis=0, tiled=True),
        lax.all_gather(rnn_gate_w, "sp", axis=0, tiled=True),
    )
    piece = lax.all_gather(normed, "tp", axis=0, tiled=True)
    joined = jnp.concatenate(
        [
            jnp.dot(piece, weight, preferred_element_type=jnp.float32).astype(jnp.bfloat16)
            for weight in gathered
        ],
        axis=1,
    )
    conv_value, conv_gate, rnn_input, rnn_gate = [
        joined[:, edges[index] : edges[index + 1]] for index in range(4)
    ]
    out_weights = (
        lax.all_gather(conv_out_w, "sp", axis=1, tiled=True),
        lax.all_gather(rnn_out_w, "sp", axis=1, tiled=True),
    )
    length = conv_value.shape[0]
    conv_reach = conv_kernel.shape[0] - 1
    short_reach = short_kernel.shape[0] - 1
    value_tail, gate_tail, input_tail = shifted(
        (
            conv_value[length - conv_reach :],
            conv_gate[length - conv_reach :],
            rnn_input[length - short_reach :],
        ),
        "sp",
        1,
    )
    value_ext = jnp.concatenate([value_tail, conv_value], axis=0)
    gate_ext = jnp.concatenate([gate_tail, conv_gate], axis=0)
    input_ext = jnp.concatenate([input_tail, rnn_input], axis=0)
    gated_values = value_ext.astype(jnp.float32) * jax.nn.sigmoid(gate_ext.astype(jnp.float32))
    conv_mixed = causal_taps(gated_values, conv_kernel, length)
    moments = lax.psum(
        (jnp.sum(conv_mixed, axis=1), jnp.sum(conv_mixed * conv_mixed, axis=1)), "tp"
    )
    channels = conv_mixed.shape[1] * lax.axis_size("tp")
    average = moments[0][:, None] / channels
    spread = moments[1][:, None] / channels - average * average
    scaled = (conv_mixed - average) * lax.rsqrt(spread + EPS)
    scaled = scaled * conv_norm_gain.astype(jnp.float32) + conv_norm_shift.astype(jnp.float32)
    conv_hidden = jax.nn.silu(scaled).astype(jnp.bfloat16)
    rnn_short = causal_taps(input_ext.astype(jnp.float32), short_kernel, length).astype(
        jnp.bfloat16
    )
    recur_gate = jax.nn.sigmoid(block_diagonal(rnn_short, recur_map))
    input_gate = jax.nn.sigmoid(block_diagonal(rnn_short, input_map))
    shift_cols = jnp.repeat(decay_shift, recur_map.shape[1], axis=1)
    log_decay = -EXPONENT * recur_gate * jax.nn.softplus(-decay_param)[None, :] + shift_cols
    drive = jnp.sqrt(-jnp.expm1(2.0 * log_decay)) * input_gate * rnn_short.astype(jnp.float32)
    cum_decay, cum_drive = lax.associative_scan(linear_pair, (jnp.exp(log_decay), drive), axis=0)
    last_decay = cum_decay[length - 1]
    last_drive = cum_drive[length - 1]
    before = entering_2(
        (last_decay, last_drive),
        "sp",
        linear_pair,
        (jnp.ones_like(last_decay), jnp.zeros_like(last_drive)),
    )
    entering = before[0] * initial_state + before[1]
    states = cum_drive + cum_decay * entering[None, :]
    rnn_hidden = (states * jax.nn.gelu(rnn_gate.astype(jnp.float32), approximate=True)).astype(
        jnp.bfloat16
    )
    return lax.psum_scatter(
        (
            jnp.dot(conv_hidden, out_weights[0], preferred_element_type=jnp.float32)
            + jnp.dot(rnn_hidden, out_weights[1], preferred_element_type=jnp.float32)
        ).astype(jnp.bfloat16),
        "tp",
        scatter_dimension=0,
        tiled=True,
    )


def solution(mesh):
    return jax.shard_map(
        local,
        mesh=mesh,
        in_specs=(
            P(("sp", "tp"), None),
            P(),
            P("sp", "tp"),
            P("sp", "tp"),
            P("sp", "tp"),
            P("sp", "tp"),
            P(None, "tp"),
            P("tp"),
            P("tp"),
            P(None, "tp"),
            P("tp", None, None),
            P("tp", None, None),
            P("tp"),
            P("sp", "tp"),
            P("tp"),
            P("tp", "sp"),
            P("tp", "sp"),
        ),
        out_specs=P(("sp", "tp"), None),
        check_vma=False,
    )
```

profile of v0, /device:TPU:0, one launch (start us, length us, event | category | flops | bytes accessed | tf_op | source)
XLA Modules:
  0.0 506.4 jit_solution(6484837186567782956)
XLA Ops:
  15.4 1.9 copy.34
  18.4 48.3 %all-gather.18.cloned.1.call-done = bf16[2048,640]{1,0:T(8,128)(2,1)} async-done(((bf16[256,640]{1,0:T(8,128)(2,1)}), bf16[2048,640]{1,0:T(8,128)(2,1)}) %all-gather.18.cloned.1.call-update) | async-done | bytes 2621456 | tf_op jit(solution)/shard_map/all_gather | solution.py:75
  66.7 28.7 %all-gather.10.cloned.1.call-done = bf16[768,2048]{1,0:T(8,128)(2,1)} async-done(((bf16[192,2048]{1,0:T(8,128)(2,1)}), bf16[768,2048]{1,0:T(8,128)(2,1)}) %all-gather.10.cloned.1.call-update) | async-done | bytes 3145744 | tf_op jit(solution)/shard_map/all_gather | solution.py:78
  95.4 5.3 %convolution_convert_fusion.1 = bf16[768,640]{1,0:T(8,128)(2,1)S(1)} fusion(bf16[768,2048]{1,0:T(8,128)(2,1)} %all-gather.10.cloned.1.call-done, bf16[2048,640]{1,0:T(8,128)(2,1)} %all-gather.18.cloned.1.call-done), kind=kOutput, calls=%fused_computation.97 | convolution fusion | flops 2013757440 | bytes 6750208 | tf_op jit(solution)/shard_map/dot_general | solution.py:81
  100.7 3.4 collective-permute-start.2
  104.0 42.6 %all-gather.12.cloned.1.call-done = bf16[2048,512]{1,0:T(8,128)(2,1)} async-done(((bf16[256,512]{1,0:T(8,128)(2,1)}), bf16[2048,512]{1,0:T(8,128)(2,1)}) %all-gather.12.cloned.1.call-update) | async-done | bytes 2097168 | tf_op jit(solution)/shard_map/all_gather | solution.py:73
  146.6 4.3 convolution_convert_fusion.3
  152.4 3.1 collective-permute-start
  155.5 40.9 %all-gather.14.cloned.1.call-done = bf16[2048,512]{1,0:T(8,128)(2,1)} async-done(((bf16[256,512]{1,0:T(8,128)(2,1)}), bf16[2048,512]{1,0:T(8,128)(2,1)}) %all-gather.14.cloned.1.call-update) | async-done | bytes 2097168 | tf_op jit(solution)/shard_map/all_gather | solution.py:74
  196.4 4.3 convolution_convert_fusion.2
  201.4 3.1 collective-permute-start.1
  207.1 3.2 add_divide_fusion.1
  210.3 2.9 copy.33
  213.2 2.0 add_divide_fusion
  215.3 2.9 copy.36
  218.1 7.0 %convert_multiply_fusion.3 = (f32[768,640]{1,0:T(8,128)}, f32[768,640]{1,0:T(8,128)}) fusion(f32[768,640]{1,0:T(8,128)} %copy.36, f32[768,640]{1,0:T(8,128)} %copy.34, f32[768,640]{1,0:T(8,128)} %copy.33, f32[640]{0:T(1024)S(1)} %fusion.63, f32[771,640]{1,0:T(8,128)S(1)} %maximum_convert_fusion, f32[640]{0:T(1024)S(1)} %get-tuple-element.45, ...), kind=kLoop, calls=%fused_computation.23 | loop fusion | flops 7372800 | bytes 17707520 | tf_op jit(solution)/shard_map/mul | solution.py:126
  225.2 5.5 %slice.567 = f32[384,640]{1,0:T(8,128)} slice(f32[768,640]{1,0:T(8,128)} %get-tuple-element.70), slice={[0:767:2], [0:640:1]} | slice | bytes 1966080 | tf_op jit(solution)/shard_map/slice | solution.py:127
  230.7 5.4 %slice.568 = f32[384,640]{1,0:T(8,128)} slice(f32[768,640]{1,0:T(8,128)} %get-tuple-element.70), slice={[1:768:2], [0:640:1]} | slice | bytes 1966080 | tf_op jit(solution)/shard_map/slice | solution.py:127
  236.1 2.8 slice.566
  238.9 2.8 slice.570
  241.7 3.3 multiply_add_fusion.2
  245.0 3.3 slice.573
  248.2 3.3 slice.574
  254.4 2.5 multiply_add_fusion.3
  256.9 1.7 slice.579
  258.6 1.8 slice.580
  260.4 1.8 slice.578
  262.2 1.7 slice.582
  268.0 1.8 multiply_add_fusion.5
  276.0 1.6 multiply_add_fusion.6
  311.3 1.7 slice.628
  317.1 3.3 slice.630
  322.3 3.0 slice.565
  325.3 5.4 %slice.632 = f32[383,640]{1,0:T(8,128)} slice(f32[768,640]{1,0:T(8,128)} %get-tuple-element.70), slice={[2:768:2], [0:640:1]} | slice | bytes 1960960 | tf_op jit(solution)/shard_map/slice | solution.py:127
  338.9 3.4 pad.127
  342.3 1.9 pad_maximum_fusion.3
  345.4 3.2 pad.143
  348.6 2.4 add.446
  352.5 3.5 pad.126
  356.9 30.4 %all-gather.1 = f32[8,1,640]{2,1,0:T(1,128)S(1)} all-gather(f32[1,1,640]{2,1,0:T(1,128)S(1)} %add_bitcast_fusion), channel_id=1, replica_groups=mesh['sp'=8,'tp'=4] {'sp'}, dimensions={0}, use_global_device_ids=true | all-gather | bytes 23040 | tf_op jit(solution)/shard_map/all_gather | solution.py:18
  387.3 3.5 pad.145
  390.9 3.7 pad.144
  395.4 30.6 %all-gather = f32[8,1,640]{2,1,0:T(1,128)S(1)} all-gather(f32[1,1,640]{2,1,0:T(1,128)S(1)} %add_bitcast_fusion.1), channel_id=1, replica_groups=mesh['sp'=8,'tp'=4] {'sp'}, dimensions={0}, use_global_device_ids=true | all-gather | bytes 23040 | tf_op jit(solution)/shard_map/all_gather | solution.py:18
  426.1 14.3 %fusion.51 = f32[768,2048]{1,0:T(8,128)} fusion(bf16[640,2048]{1,0:T(8,128)(2,1)} %all-gather.22.cloned.1.call-done, f32[768,640]{1,0:T(8,128)} %pad.144, f32[768,640]{1,0:T(8,128)} %pad.145, f32[768,640]{1,0:T(8,128)} %pad.126, f32[768,640]{1,0:T(8,128)} %pad.127, bf16[768,2048]{1,0:T(8,128)(2,1)} %all-gather.10.cloned.1.call-done, ...), kind=kOutput, calls=%fused_computation.113 | convolution fusion | flops 4034396160 | bytes 22546944 | tf_op jit(solution)/shard_map/dot_general | solution.py:144
  442.5 6.8 %fusion.69 = (f32[768]{0:T(1024)S(1)}, f32[768]{0:T(1024)S(1)}, f32[768,512]{1,0:T(8,128)S(1)}) fusion(f32[798,512]{1,0:T(8,128)S(1)} %divide_multiply_fusion, f32[512]{0:T(512)S(1)} %bitcast.99, f32[512]{0:T(512)S(1)} %bitcast.100, f32[512]{0:T(512)S(1)} %bitcast.71, f32[512]{0:T(512)S(1)} %bitcast.72, f32[512]{0:T(512)S(1)} %bitcast.73, ...), kind=kLoop, calls=%fused_computation.218 | loop fusion | flops 25164288 | bytes 50401280 | tf_op jit(solution)/shard_map/reduce_sum | solution.py:111
  449.3 5.8 %all-reduce.36 = (f32[768]{0:T(1024)S(1)}, f32[768]{0:T(1024)S(1)}) all-reduce(f32[768]{0:T(1024)S(1)} %get-tuple-element.42, f32[768]{0:T(1024)S(1)} %get-tuple-element.41), channel_id=1, replica_groups=mesh['sp'=8,'tp'=4] {'tp'}, use_global_device_ids=true, to_apply=%region_4.0 | all-reduce | flops 1536 | bytes 12288 | tf_op jit(solution)/shard_map/psum | solution.py:110
  455.1 7.3 %add_convert_fusion = bf16[768,2048]{1,0:T(8,128)(2,1)} fusion(f32[768,2048]{1,0:T(8,128)} %fusion.51, bf16[512,2048]{1,0:T(8,128)(2,1)} %all-gather.16.cloned.1.call-done, f32[768,512]{1,0:T(8,128)S(1)} %get-tuple-element.61, f32[512]{0:T(512)S(1)} %copy-done.81, f32[512]{0:T(512)S(1)} %copy-done.80, f32[768]{0:T(1024)S(1)} %get-tuple-element.140, ...), kind=kOutput, calls=%fused_computation.3 | convolution fusion | flops 1617297408 | bytes 13117440 | tf_op jit(solution)/shard_map/dot_general | solution.py:143
  462.4 37.1 %reduce-scatter.2.cloned.1.call-done = bf16[192,2048]{1,0:T(8,128)(2,1)} async-done(((bf16[768,2048]{1,0:T(8,128)(2,1)}), bf16[192,2048]{1,0:T(8,128)(2,1)}) %reduce-scatter.2.cloned.1.call-update) | async-done | bytes 786448 | tf_op jit(solution)/shard_map/reduce_scatter | solution.py:141
  (341 shorter events, 81.0 us)
Async XLA Ops:
  6.5 200.5 %copy-start = (bf16[4,160,160]{2,1,0:T(8,128)(2,1)S(1)}, bf16[4,160,160]{2,1,0:T(8,128)(2,1)}, u32[]{:S(2)}) copy-start(bf16[4,160,160]{2,1,0:T(8,128)(2,1)} %param.29) | copy-start | bytes 614404
  6.5 2.8 copy-start.8
  6.5 60.1 %all-gather.18.cloned.1.call-start = ((), (), s32[]{:S(2)}) async-start(), calls=%async_computation.5 | async-start | bytes 2949120 | tf_op jit(solution)/shard_map/all_gather | solution.py:75
  7.3 88.1 %all-gather.10.cloned.1.call-start = ((), (), s32[]{:S(2)}) async-start(), calls=%async_computation.1 | async-start | bytes 3932160 | tf_op jit(solution)/shard_map/all_gather | solution.py:78
  9.4 4.5 copy-start.22
  9.4 5.8 %copy-start.29 = (bf16[4,640]{1,0:T(4,128)(2,1)S(1)}, bf16[4,640]{1,0:T(4,128)(2,1)}, u32[]{:S(2)}) copy-start(bf16[4,640]{1,0:T(4,128)(2,1)} %param.28) | copy-start | bytes 15364
  9.4 5.8 %copy-start.30 = (f32[768,4]{0,1:T(4,128)S(1)}, f32[768,4]{0,1:T(4,128)}, u32[]{:S(2)}) copy-start(f32[768,4]{0,1:T(4,128)} %param.32) | copy-start | bytes 36868
  10.6 136.0 %all-gather.12.cloned.1.call-start = ((), (), s32[]{:S(2)}) async-start(), calls=%async_computation.2 | async-start | bytes 2359296 | tf_op jit(solution)/shard_map/all_gather | solution.py:73
  11.3 185.0 %all-gather.14.cloned.1.call-start = ((), (), s32[]{:S(2)}) async-start(), calls=%async_computation.3 | async-start | bytes 2359296 | tf_op jit(solution)/shard_map/all_gather | solution.py:74
  11.9 414.2 %all-gather.20.cloned.1.call-start = ((), (), s32[]{:S(2)}) async-start(), calls=%async_computation.6 | async-start | bytes 2949120 | tf_op jit(solution)/shard_map/all_gather | solution.py:76
  12.5 413.7 %all-gather.22.cloned.1.call-start = ((), (), s32[]{:S(2)}) async-start(), calls=%async_computation.7 | async-start | bytes 2949120 | tf_op jit(solution)/shard_map/all_gather | solution.py:91
  13.0 442.0 %all-gather.16.cloned.1.call-start = ((), (), s32[]{:S(2)}) async-start(), calls=%async_computation.4 | async-start | bytes 2359296 | tf_op jit(solution)/shard_map/all_gather | solution.py:90
  13.8 485.8 %reduce-scatter.2.cloned.1.call-start = ((), (), s32[]{:S(2)}) async-start(), calls=%async_computation.8 | async-start | bytes 3932160 | tf_op jit(solution)/shard_map/reduce_scatter | solution.py:141
  15.4 2.4 copy-start.83
  100.7 103.8 %collective-permute-start.2 = (bf16[3,640]{1,0:T(4,128)(2,1)S(1)}, bf16[3,640]{1,0:T(4,128)(2,1)S(1)}, u32[]{:S(2)}, u32[]{:S(2)}) collective-permute-start(bf16[3,640]{1,0:T(4,128)(2,1)S(1)} %slice.685), channel_id=1, source_target_pairs={{0,4},{4,8},{8,12},{12,16},{16,20},{20,24},{24,28},{1,5},{5,9},{9,... | collective-permute-start | bytes 11528 | tf_op jit(solution)/shard_map/ppermute | solution.py:13
  152.4 288.3 %collective-permute-start = (bf16[30,512]{1,0:T(8,128)(2,1)}, bf16[30,512]{1,0:T(8,128)(2,1)}, u32[]{:S(2)}, u32[]{:S(2)}) collective-permute-start(bf16[30,512]{1,0:T(8,128)(2,1)} %slice.652), channel_id=1, source_target_pairs={{0,4},{4,8},{8,12},{12,16},{16,20},{20,24},{24,28},{1,5},{5,9},{9,... | collective-permute-start | bytes 92168 | tf_op jit(solution)/shard_map/ppermute | solution.py:13
  200.7 4.0 copy-start.15
  201.4 239.4 %collective-permute-start.1 = (bf16[30,512]{1,0:T(8,128)(2,1)}, bf16[30,512]{1,0:T(8,128)(2,1)}, u32[]{:S(2)}, u32[]{:S(2)}) collective-permute-start(bf16[30,512]{1,0:T(8,128)(2,1)} %slice.653), channel_id=1, source_target_pairs={{0,4},{4,8},{8,12},{12,16},{16,20},{20,24},{24,28},{1,5},{5,9},{9,... | collective-permute-start | bytes 92168 | tf_op jit(solution)/shard_map/ppermute | solution.py:13
  210.3 3.0 copy-start.11
  210.3 3.0 copy-start.84
  225.2 10.9 %copy-start.2 = (f32[768,640]{1,0:T(8,128)S(1)}, f32[768,640]{1,0:T(8,128)}, u32[]{:S(2)}) copy-start(f32[768,640]{1,0:T(8,128)} %get-tuple-element.71) | copy-start | bytes 5898244
  322.3 10.4 %copy-start.24 = (f32[3,640]{1,0:T(4,128)S(1)}, f32[3,640]{1,0:T(4,128)}, u32[]{:S(2)}) copy-start(f32[3,640]{1,0:T(4,128)} %slice.610) | copy-start | bytes 23044
  322.3 10.4 %copy-start.25 = (f32[3,640]{1,0:T(4,128)S(1)}, f32[3,640]{1,0:T(4,128)}, u32[]{:S(2)}) copy-start(f32[3,640]{1,0:T(4,128)} %slice.608) | copy-start | bytes 23044
  322.3 10.4 %copy-start.26 = (f32[3,640]{1,0:T(4,128)S(1)}, f32[3,640]{1,0:T(4,128)}, u32[]{:S(2)}) copy-start(f32[3,640]{1,0:T(4,128)} %slice.612) | copy-start | bytes 23044
  322.3 10.5 %copy-start.27 = (f32[2,640]{1,0:T(2,128)S(1)}, f32[2,640]{1,0:T(2,128)}, u32[]{:S(2)}) copy-start(f32[2,640]{1,0:T(2,128)} %slice.607) | copy-start | bytes 15364
  322.3 10.5 %copy-start.28 = (f32[2,640]{1,0:T(2,128)S(1)}, f32[2,640]{1,0:T(2,128)}, u32[]{:S(2)}) copy-start(f32[2,640]{1,0:T(2,128)} %slice.618) | copy-start | bytes 15364
  322.3 10.5 %copy-start.39 = (f32[1,640]{1,0:T(1,128)S(1)}, f32[1,640]{1,0:T(1,128)}, u32[]{:S(2)}) copy-start(f32[1,640]{1,0:T(1,128)} %slice.697) | copy-start | bytes 7684
  322.3 10.5 %copy-start.40 = (f32[1,640]{1,0:T(1,128)S(1)}, f32[1,640]{1,0:T(1,128)}, u32[]{:S(2)}) copy-start(f32[1,640]{1,0:T(1,128)} %slice.726) | copy-start | bytes 7684
  325.3 7.7 %copy-start.23 = (f32[5,640]{1,0:T(8,128)S(1)}, f32[5,640]{1,0:T(8,128)}, u32[]{:S(2)}) copy-start(f32[5,640]{1,0:T(8,128)} %slice.620) | copy-start | bytes 38404
  325.3 7.7 %copy-start.42 = (f32[1,640]{1,0:T(1,128)S(1)}, f32[1,640]{1,0:T(1,128)}, u32[]{:S(2)}) copy-start(f32[1,640]{1,0:T(1,128)} %slice.725) | copy-start | bytes 7684
  325.3 7.8 %copy-start.41 = (f32[1,640]{1,0:T(1,128)S(1)}, f32[1,640]{1,0:T(1,128)}, u32[]{:S(2)}) copy-start(f32[1,640]{1,0:T(1,128)} %slice.696) | copy-start | bytes 7684
  325.3 7.9 %copy-start.20 = (f32[11,640]{1,0:T(8,128)S(1)}, f32[11,640]{1,0:T(8,128)}, u32[]{:S(2)}) copy-start(f32[11,640]{1,0:T(8,128)} %slice.595) | copy-start | bytes 84484
  325.3 7.9 %copy-start.21 = (f32[11,640]{1,0:T(8,128)S(1)}, f32[11,640]{1,0:T(8,128)}, u32[]{:S(2)}) copy-start(f32[11,640]{1,0:T(8,128)} %slice.622) | copy-start | bytes 84484
  325.3 7.9 %copy-start.46 = (f32[1,640]{1,0:T(1,128)S(1)}, f32[1,640]{1,0:T(1,128)}, u32[]{:S(2)}) copy-start(f32[1,640]{1,0:T(1,128)} %slice.724) | copy-start | bytes 7684
  325.3 8.0 %copy-start.45 = (f32[1,640]{1,0:T(1,128)S(1)}, f32[1,640]{1,0:T(1,128)}, u32[]{:S(2)}) copy-start(f32[1,640]{1,0:T(1,128)} %slice.695) | copy-start | bytes 7684
  330.8 2.6 copy-start.19
  330.8 2.7 copy-start.44
  338.9 3.5 copy-start.33
  348.6 2.4 copy-start.6
  352.5 34.8 %copy-start.7 = (f32[384,640]{1,0:T(8,128)S(1)}, f32[384,640]{1,0:T(8,128)}, u32[]{:S(2)}) copy-start(f32[384,640]{1,0:T(8,128)} %add.446) | copy-start | bytes 2949124
  356.1 34.8 %copy-start.4 = (f32[383,640]{1,0:T(8,128)S(1)}, f32[383,640]{1,0:T(8,128)}, u32[]{:S(2)}) copy-start(f32[383,640]{1,0:T(8,128)} %get-tuple-element.73) | copy-start | bytes 2941444
  356.1 34.8 %copy-start.31 = (f32[1,640]{1,0:T(1,128)S(1)}, f32[1,640]{1,0:T(1,128)}, u32[]{:S(2)}) copy-start(f32[1,640]{1,0:T(1,128)} %slice.719) | copy-start | bytes 7684
  390.9 35.1 %copy-start.79 = (f32[640]{0:T(1024)S(1)}, f32[640]{0:T(1024)}, u32[]{:S(2)}) copy-start(f32[640]{0:T(1024)} %param.33) | copy-start | bytes 7684
  426.1 14.7 %copy-start.14 = (bf16[768,512]{1,0:T(8,128)(2,1)S(1)}, bf16[768,512]{1,0:T(8,128)(2,1)}, u32[]{:S(2)}) copy-start(bf16[768,512]{1,0:T(8,128)(2,1)} %copy-done.13) | copy-start | bytes 2359300
  426.1 14.7 %copy-start.16 = (bf16[768,512]{1,0:T(8,128)(2,1)S(1)}, bf16[768,512]{1,0:T(8,128)(2,1)}, u32[]{:S(2)}) copy-start(bf16[768,512]{1,0:T(8,128)(2,1)} %copy-done.15) | copy-start | bytes 2359300
  442.5 12.6 %copy-start.80 = (f32[512]{0:T(512)S(1)}, f32[512]{0:T(512)}, u32[]{:S(2)}) copy-start(f32[512]{0:T(512)} %convert_element_type.131) | copy-start | bytes 6148
  442.5 12.6 %copy-start.81 = (f32[512]{0:T(512)S(1)}, f32[512]{0:T(512)}, u32[]{:S(2)}) copy-start(f32[512]{0:T(512)} %convert_element_type.132) | copy-start | bytes 6148
  455.1 44.5 %copy-start.1 = (bf16[4,160,160]{2,1,0:T(8,128)(2,1)S(1)}, bf16[4,160,160]{2,1,0:T(8,128)(2,1)}, u32[]{:S(2)}) copy-start(bf16[4,160,160]{2,1,0:T(8,128)(2,1)} %param.29) | copy-start | bytes 614404
  (48 other events, 74.2 us)
Sparse Core Ops, SparseCore 0:
  9.5 57.1 all-gather.17
  68.2 27.0 all-gather.9
  97.5 49.0 all-gather.11
  148.6 47.7 all-gather.13
  198.4 52.9 all-gather.19
  253.2 56.1 all-gather.21
  311.5 48.5 all-gather.15
  462.6 36.9 reduce-scatter.1
where the time goes:
time: 509 us; the launch traced here: 506 us
  waiting for transfers between devices  201 us (39%)
  local copies, waits for them, and re-layouts  128 us (25%)
  blocking collectives  66.8 us (13%)
  other arithmetic  44.8 us (9%)
  matrix products  40.8 us (8%)
  between operations  15.1 us (3%)
  starting transfers between devices  9.79 us (2%)
    slice x64, local copies, waits for them, and re-layouts, local(): lax.associative_scan(linear_pair, (jnp.exp(log_decay), drive), axis=0)  94.5 us
    all_gather x2, blocking collectives, entering_2(): gathered = jax.tree.map(lambda a: lax.all_gather(a, axis), part)  61.1 us
    all_gather x1, waiting for transfers between devices, local(): lax.all_gather(rnn_input_w, 'sp', axis=0, tiled=True)  48.3 us
    all_gather x1, waiting for transfers between devices, local(): lax.all_gather(conv_value_w, 'sp', axis=0, tiled=True)  42.6 us
    all_gather x1, waiting for transfers between devices, local(): lax.all_gather(conv_gate_w, 'sp', axis=0, tiled=True)  40.9 us
    reduce_scatter x1, waiting for transfers between devices, local(): lax.psum_scatter((jnp.dot(conv_hidden, out_weights[0], preferred_element_...  37.1 us
    all_gather x1, waiting for transfers between devices, local(): piece = lax.all_gather(normed, 'tp', axis=0, tiled=True)  28.7 us
    pad x34, local copies, waits for them, and re-layouts, local(): lax.associative_scan(linear_pair, (jnp.exp(log_decay), drive), axis=0)  19.5 us
  transfers between devices with their start and end apart: 11, of which 5 were waited for; matrix products, arithmetic and copies ran while one was open for 40% of the time, Pallas kernels for 0%

commit v1 on v0

--- a/solution.py
+++ b/solution.py
@@ -1,6 +1,10 @@
+import functools
+
 import jax
 import jax.numpy as jnp
 from jax import lax
+from jax.experimental import pallas as pl
+from jax.experimental.pallas import tpu as pltpu
 from jax.sharding import PartitionSpec as P
 
 EPS = 1e-06
@@ -13,17 +17,248 @@
     return lax.ppermute(x, axis, pairs)
 
 
-def entering_2(part, axis, combine, identity):
-    place = lax.axis_index(axis)
-    gathered = jax.tree.map(lambda a: lax.all_gather(a, axis), part)
-    state = jax.tree.map(lambda a, e: jnp.zeros_like(a) + jnp.asarray(e, a.dtype), part, identity)
-
-    def one(step, state):
-        return combine(
-            state, jax.tree.map(lambda a: lax.dynamic_index_in_dim(a, step, 0, False), gathered)
+def send_to(src, dst, send, recv, axis, peer):
+    return pltpu.make_async_remote_copy(
+        src_ref=src,
+        dst_ref=dst,
+        send_sem=send,
+        recv_sem=recv,
+        device_id={axis: peer},
+        device_id_type=pl.DeviceIdType.MESH,
+    )
+
+
+def project_kernel(n, m, x_ref, w_ref, o_ref, blocks, piece, acc, ring_send, ring_recv, tok_send, tok_recv, own_sem):
+    half = n // 2
+    me = lax.axis_index("sp")
+    lane = lax.axis_index("tp")
+    at = jnp.where(me % 2 == 0, me // 2, n - 1 - me // 2)
+
+    def device_at(place):
+        place = lax.rem(place + 2 * n, n)
+        return jnp.where(place < half, 2 * place, 2 * (n - 1 - place) + 1)
+
+    right = device_at(at + 1)
+    left = device_at(at - 1)
+    barrier = pltpu.get_barrier_semaphore()
+    for peer in (left, right):
+        pl.semaphore_signal(barrier, inc=1, device_id={"sp": peer}, device_id_type=pl.DeviceIdType.MESH)
+    for i in range(1, m):
+        pl.semaphore_signal(
+            barrier, inc=1, device_id={"tp": lax.rem(lane + i, m)}, device_id_type=pl.DeviceIdType.MESH
         )
-
-    return lax.fori_loop(0, place, one, state)
+    own_w = pltpu.make_async_copy(w_ref, blocks.at[me], own_sem.at[0])
+    own_x = pltpu.make_async_copy(x_ref, piece.at[lane], own_sem.at[1])
+    own_w.start()
+    own_x.start()
+    own_w.wait()
+    own_x.wait()
+    pl.semaphore_wait(barrier, 2 + m - 1)
+    rows = w_ref.shape[0] // 2
+
+    def hop(way, k, part=None):
+        slot = device_at(at - (k - 1)) if way == 0 else device_at(at + (k - 1))
+        ref = blocks.at[slot] if part is None else blocks.at[slot, pl.ds(part * rows, rows)]
+        return send_to(
+            ref, ref, ring_send.at[way, k - 1], ring_recv.at[way, k - 1], "sp", right if way == 0 else left
+        )
+
+    tokens_out = [
+        send_to(x_ref, piece.at[lane], tok_send.at[i - 1], tok_recv.at[i - 1], "tp", lax.rem(lane + i, m))
+        for i in range(1, m)
+    ]
+
+    def add(slot, first=False):
+        def one(j, _):
+            here = pl.ds(pl.multiple_of(j * piece.shape[2], piece.shape[2]), piece.shape[2])
+            term = jnp.dot(piece[j, slot], blocks[slot], preferred_element_type=jnp.float32)
+            acc[here, :] = term if first else acc[here, :] + term
+            return 0
+
+        lax.fori_loop(0, m, one, 0)
+
+    hop(0, 1).start()
+    hop(1, 1).start()
+    for copy in tokens_out:
+        copy.start()
+    hop(0, 1).wait_recv()
+    hop(1, 1).wait_recv()
+    hop(0, 2).start()
+    hop(1, 2).start()
+    for copy in tokens_out:
+        copy.wait_recv()
+    add(me, True)
+
+    def step(k, _):
+        add(device_at(at - (k - 1)))
+        add(device_at(at + (k - 1)))
+        hop(0, k).wait_recv()
+        hop(1, k).wait_recv()
+
+        @pl.when(k + 1 < half)
+        def _():
+            hop(0, k + 1).start()
+            hop(1, k + 1).start()
+
+        return 0
+
+    lax.fori_loop(2, half, step, 0)
+    hop(0, half, 0).start()
+    hop(1, half, 1).start()
+    add(device_at(at - (half - 1)))
+    add(device_at(at + (half - 1)))
+    hop(0, half, 0).wait_recv()
+    hop(1, half, 1).wait_recv()
+    add(device_at(at + half))
+
+    def finish(j, _):
+        here = pl.ds(pl.multiple_of(j * piece.shape[2], piece.shape[2]), piece.shape[2])
+        o_ref[here, :] = acc[here, :].astype(o_ref.dtype)
+        return 0
+
+    lax.fori_loop(0, m, finish, 0)
+
+    def sent(k, _):
+        hop(0, k).wait_send()
+        hop(1, k).wait_send()
+        return 0
+
+    lax.fori_loop(1, half, sent, 0)
+    hop(0, half, 0).wait_send()
+    hop(1, half, 1).wait_send()
+    for copy in tokens_out:
+        copy.wait_send()
+
+
+def project(normed, weight):
+    n = lax.axis_size("sp")
+    m = lax.axis_size("tp")
+    rows = normed.shape[0]
+    depth, columns = weight.shape
+    sliced = normed.reshape(rows, n, depth).transpose(1, 0, 2)
+    vmem = pl.BlockSpec(memory_space=pltpu.VMEM)
+    return pl.pallas_call(
+        functools.partial(project_kernel, n, m),
+        out_shape=jax.ShapeDtypeStruct((rows * m, columns), jnp.bfloat16),
+        in_specs=[vmem, vmem],
+        out_specs=vmem,
+        scratch_shapes=[
+            pltpu.VMEM((n, depth, columns), jnp.bfloat16),
+            pltpu.VMEM((m, n, rows, depth), jnp.bfloat16),
+            pltpu.VMEM((rows * m, columns), jnp.float32),
+            pltpu.SemaphoreType.DMA((2, n // 2)),
+            pltpu.SemaphoreType.DMA((2, n // 2)),
+            pltpu.SemaphoreType.DMA((m - 1,)),
+            pltpu.SemaphoreType.DMA((m - 1,)),
+            pltpu.SemaphoreType.DMA((2,)),
+        ],
+        cost_estimate=pl.CostEstimate(
+            flops=2 * rows * m * depth * n * columns, bytes_accessed=90_000_000, transcendentals=0
+        ),
+        compiler_params=pltpu.CompilerParams(
+            collective_id=0, has_side_effects=True, vmem_limit_bytes=50 * 1024 * 1024
+        ),
+    )(sliced, weight)
+
+
+def spread_kernel(n, axis, x_ref, o_ref, send, recv):
+    me = lax.axis_index(axis)
+    barrier = pltpu.get_barrier_semaphore()
+
+    def greet(i, _):
+        pl.semaphore_signal(
+            barrier, inc=1, device_id={axis: lax.rem(me + i, n)}, device_id_type=pl.DeviceIdType.MESH
+        )
+        return 0
+
+    lax.fori_loop(1, n, greet, 0)
+    pl.semaphore_wait(barrier, n - 1)
+
+    def copy(i):
+        return send_to(x_ref, o_ref.at[me], send.at[i - 1], recv.at[i - 1], axis, lax.rem(me + i, n))
+
+    def start(i, _):
+        copy(i).start()
+        return 0
+
+    def wait(i, _):
+        copy(i).wait()
+        return 0
+
+    lax.fori_loop(1, n, start, 0)
+    o_ref[pl.ds(me, 1)] = x_ref[...][None]
+    lax.fori_loop(1, n, wait, 0)
+
+
+def spread_over(x, axis, collective_id):
+    n = lax.axis_size(axis)
+    vmem = pl.BlockSpec(memory_space=pltpu.VMEM)
+    return pl.pallas_call(
+        functools.partial(spread_kernel, n, axis),
+        out_shape=jax.ShapeDtypeStruct((n,) + x.shape, x.dtype),
+        in_specs=[vmem],
+        out_specs=vmem,
+        scratch_shapes=[pltpu.SemaphoreType.DMA((n - 1,)), pltpu.SemaphoreType.DMA((n - 1,))],
+        cost_estimate=pl.CostEstimate(flops=0, bytes_accessed=10_000_000, transcendentals=0),
+        compiler_params=pltpu.CompilerParams(
+            collective_id=collective_id, has_side_effects=True, vmem_limit_bytes=4 * 1024 * 1024
+        ),
+    )(x)
+
+
+def scan_kernel(parts, a_ref, b_ref, p_ref, h_ref):
+    length, width = a_ref.shape
+    run = length // parts
+    cols = [slice(None)]
+
+    def one(i, state):
+        place = pl.ds(i, parts, stride=run)
+        new = []
+        for c, (p, h) in zip(cols, state):
+            a = a_ref[place, c]
+            h = a * h + b_ref[place, c]
+            p = a * p
+            p_ref[place, c] = p
+            h_ref[place, c] = h
+            new.append((p, h))
+        return new
+
+    first = [(jnp.ones((parts, width), jnp.float32), jnp.zeros((parts, width), jnp.float32)) for _ in cols]
+    ends = lax.fori_loop(0, run, one, first)
+    for c, (p, h) in zip(cols, ends):
+        carry_p = p[0:1]
+        carry_h = h[0:1]
+        for s in range(1, parts):
+            here = pl.ds(s * run, run)
+            local_p = p_ref[here, c]
+            h_ref[here, c] = h_ref[here, c] + local_p * carry_h
+            p_ref[here, c] = local_p * carry_p
+            carry_h = p[s : s + 1] * carry_h + h[s : s + 1]
+            carry_p = p[s : s + 1] * carry_p
+
+
+def scan(a, b):
+    block = pl.BlockSpec((a.shape[0], 128), lambda c: (0, c))
+    return pl.pallas_call(
+        functools.partial(scan_kernel, 8),
+        grid=(a.shape[1] // 128,),
+        out_shape=[jax.ShapeDtypeStruct(a.shape, jnp.float32)] * 2,
+        in_specs=[block, block],
+        out_specs=[block, block],
+        cost_estimate=pl.CostEstimate(flops=4 * a.size, bytes_accessed=16 * a.size, transcendentals=0),
+        compiler_params=pltpu.CompilerParams(vmem_limit_bytes=20 * 1024 * 1024),
+    )(a, b)
+
+
+def entering(last_decay, last_drive, initial):
+    n = lax.axis_size("sp")
+    place = lax.axis_index("sp")
+    pair = jnp.stack([last_decay, last_drive])
+    gathered = spread_over(jnp.pad(pair, ((0, 6), (0, 0))), "sp", 1)
+    state = initial
+    for i in range(n):
+        state = jnp.where(i < place, gathered[i, 0] * state + gathered[i, 1], state)
+    return state
 
 
 def causal_taps(extended, kernel, length):
@@ -33,15 +268,12 @@
     return result
 
 
-def linear_pair(earlier, later):
-    return (earlier[0] * later[0], later[0] * earlier[1] + later[1])
-
-
 def block_diagonal(values, maps):
-    row_count = values.shape[0]
-    grouped = values.reshape(row_count, maps.shape[0], maps.shape[1])
-    mapped = jnp.einsum("rhi,hij->rhj", grouped, maps, preferred_element_type=jnp.float32)
-    return mapped.reshape(row_count, -1)
+    heads, size, _ = maps.shape
+    rows = [
+        jnp.pad(maps[h], ((0, 0), (h * size, (heads - 1 - h) * size))) for h in range(heads)
+    ]
+    return jnp.dot(values, jnp.concatenate(rows, axis=0), preferred_element_type=jnp.float32)
 
 
 def local(
@@ -69,19 +301,8 @@
     edges = [0]
     for weight in (conv_value_w, conv_gate_w, rnn_input_w, rnn_gate_w):
         edges.append(edges[-1] + weight.shape[1])
-    gathered = (
-        lax.all_gather(conv_value_w, "sp", axis=0, tiled=True),
-        lax.all_gather(conv_gate_w, "sp", axis=0, tiled=True),
-        lax.all_gather(rnn_input_w, "sp", axis=0, tiled=True),
-        lax.all_gather(rnn_gate_w, "sp", axis=0, tiled=True),
-    )
-    piece = lax.all_gather(normed, "tp", axis=0, tiled=True)
-    joined = jnp.concatenate(
-        [
-            jnp.dot(piece, weight, preferred_element_type=jnp.float32).astype(jnp.bfloat16)
-            for weight in gathered
-        ],
-        axis=1,
+    joined = project(
+        normed, jnp.concatenate([conv_value_w, conv_gate_w, rnn_input_w, rnn_gate_w], axis=1)
     )
     conv_value, conv_gate, rnn_input, rnn_gate = [
         joined[:, edges[index] : edges[index + 1]] for index in range(4)
@@ -93,15 +314,10 @@
     length = conv_value.shape[0]
     conv_reach = conv_kernel.shape[0] - 1
     short_reach = short_kernel.shape[0] - 1
-    value_tail, gate_tail, input_tail = shifted(
-        (
-            conv_value[length - conv_reach :],
-            conv_gate[length - conv_reach :],
-            rnn_input[length - short_reach :],
-        ),
-        "sp",
-        1,
-    )
+    tail = shifted(joined[length - conv_reach :, : edges[3]], "sp", 1)
+    value_tail = tail[:, : edges[1]]
+    gate_tail = tail[:, edges[1] : edges[2]]
+    input_tail = tail[conv_reach - short_reach :, edges[2] :]
     value_ext = jnp.concatenate([value_tail, conv_value], axis=0)
     gate_ext = jnp.concatenate([gate_tail, conv_gate], axis=0)
     input_ext = jnp.concatenate([input_tail, rnn_input], axis=0)
@@ -124,17 +340,9 @@
     shift_cols = jnp.repeat(decay_shift, recur_map.shape[1], axis=1)
     log_decay = -EXPONENT * recur_gate * jax.nn.softplus(-decay_param)[None, :] + shift_cols
     drive = jnp.sqrt(-jnp.expm1(2.0 * log_decay)) * input_gate * rnn_short.astype(jnp.float32)
-    cum_decay, cum_drive = lax.associative_scan(linear_pair, (jnp.exp(log_decay), drive), axis=0)
-    last_decay = cum_decay[length - 1]
-    last_drive = cum_drive[length - 1]
-    before = entering_2(
-        (last_decay, last_drive),
-        "sp",
-        linear_pair,
-        (jnp.ones_like(last_decay), jnp.zeros_like(last_drive)),
-    )
-    entering = before[0] * initial_state + before[1]
-    states = cum_drive + cum_decay * entering[None, :]
+    cum_decay, cum_drive = scan(jnp.exp(log_decay), drive)
+    state_before = entering(cum_decay[length - 1], cum_drive[length - 1], initial_state)
+    states = cum_drive + cum_decay * state_before[None, :]
     rnn_hidden = (states * jax.nn.gelu(rnn_gate.astype(jnp.float32), approximate=True)).astype(
         jnp.bfloat16
     )

time: 509 us -> 255 us (0.50)
  waiting for transfers between devices: 201 us -> 39.6 us
  Pallas kernels: 0 us -> 150 us
  local copies, waits for them, and re-layouts: 128 us -> 8.58 us
  blocking collectives: 66.8 us -> 6.34 us
  other arithmetic: 44.8 us -> 14 us
  matrix products: 40.8 us -> 18.7 us
  starting transfers between devices: 9.79 us -> 2.66 us
    all_gather x5 -> x0, waiting for transfers between devices: 160 us -> none  [the longest x1 48.3 us: local(): lax.all_gather(rnn_input_w, 'sp', axis=0, tiled=True)]
    pallas_call x0 -> x3, Pallas kernels: none -> 150 us  [the longest x1 135 us: project(): pl.pallas_call(functools.partial(project_kernel, n, m), out_shape=jax.Sha...]
    slice x67 -> x9, local copies, waits for them, and re-layouts: 95.8 us -> 3.69 us  [the longest x3 2.63 us: local(): joined[:, edges[index]:edges[index + 1]]]
    all_gather x2 -> x0, blocking collectives: 61.1 us -> none  [entering_2(): gathered = jax.tree.map(lambda a: lax.all_gather(a, axis), part)]
    pad x34 -> x0, local copies, waits for them, and re-layouts: 19.5 us -> none  [local(): lax.associative_scan(linear_pair, (jnp.exp(log_decay), drive), axis=0)]
    add x33 -> x0, other arithmetic: 19 us -> none  [the longest x17 15.5 us: linear_pair(): return (earlier[0] * later[0], later[0] * earlier[1] + later[1])]
    dot_general x5 -> x2, matrix products: 19.2 us -> 3.2 us  [block_diagonal(): jnp.dot(values, jnp.concatenate(rows, axis=0), preferred_element_type=jnp...]
    mul x1 -> x0, other arithmetic: 7.04 us -> none  [local(): jnp.sqrt(-jnp.expm1(2.0 * log_decay)) * input_gate]
  transfers between devices with their start and end apart: 11 -> 4, of which waited for: 5 -> 1; matrix products, arithmetic and copies ran while one was open for 40% -> 13% of each run, Pallas kernels for 0% -> 59%
where the time goes in v1:
time: 255 us; the launch traced here: 254 us
  Pallas kernels  150 us (59%)
  waiting for transfers between devices  39.6 us (16%)
  matrix products  18.7 us (7%)
  other arithmetic  14 us (5%)
  between operations  14 us (5%)
  local copies, waits for them, and re-layouts  8.58 us (3%)
  blocking collectives  6.34 us (2%)
  starting transfers between devices  2.66 us (1%)
    pallas_call x1, Pallas kernels, project(): pl.pallas_call(functools.partial(project_kernel, n, m), out_shape=jax.Sha...  135 us
    reduce_scatter x1, waiting for transfers between devices, local(): lax.psum_scatter((jnp.dot(conv_hidden, out_weights[0], preferred_element_...  38.8 us
    pallas_call x1, Pallas kernels, scan(): pl.pallas_call(functools.partial(scan_kernel, 8), grid=(a.shape[1] // 128...  8.72 us
    dot_general x1, matrix products, local(): jnp.dot(rnn_hidden, out_weights[1], preferred_element_type=jnp.float32)  8.31 us
    reduce_sum x1, other arithmetic, local(): jnp.sum(conv_mixed, axis=1)  7.42 us
    dot_general x1, matrix products, local(): jnp.dot(conv_hidden, out_weights[0], preferred_element_type=jnp.float32)  7.23 us
    pallas_call x1, Pallas kernels, spread_over(): pl.pallas_call(functools.partial(spread_kernel, n, axis), out_shape=jax.S...  6.84 us
    psum x1, blocking collectives, local(): lax.psum((jnp.sum(conv_mixed, axis=1), jnp.sum(conv_mixed * conv_mixed, a...  6.34 us
  transfers between devices with their start and end apart: 4, of which 1 were waited for; matrix products, arithmetic and copies ran while one was open for 13% of the time, Pallas kernels for 59%

profile of v1, /device:TPU:0, one launch (start us, length us, event | category | flops | bytes accessed | tf_op | source)
XLA Modules:
  0.0 254.4 jit_solution(17598612370740715606)
XLA Ops:
  6.5 0.7 all-gather.5.cloned.1.call-update
  7.3 0.0 all-gather.3.cloned.1.call-start
  7.3 0.7 convert_element_type.127
  8.0 1.4 fusion.17
  9.4 0.0 copy-start.6
  9.4 0.0 copy-start.10
  9.4 0.3 fusion.19
  9.7 0.1 copy.23
  9.7 0.6 copy-done.6
  10.4 0.1 copy-done.7
  10.5 0.1 copy-done.9
  10.5 0.1 copy-done.10
  10.6 0.1 pad_maximum_fusion.w_ref
  10.7 134.9 %shard_map.163 = bf16[768,2304]{1,0:T(8,128)(2,1)} custom-call(bf16[8,192,256]{2,1,0:T(8,128)(2,1)S(1)} %bitcast.59, bf16[256,2304]{1,0:T(8,128)(2,1)S(1)} %pad_maximum_fusion.w_ref), custom_call_target="tpu_custom_call" | custom-call | flops 7247757312 | bytes 90000000 | tf_op jit(solution)/shard_map/pallas_call | solution.py:140
  145.6 0.9 slice.313
  146.5 2.6 %collective-permute-start = (bf16[30,1664]{1,0:T(8,128)(2,1)S(1)}, bf16[30,1664]{1,0:T(8,128)(2,1)S(1)}, u32[]{:S(2)}, u32[]{:S(2)}) collective-permute-start(bf16[30,1664]{1,0:T(8,128)(2,1)S(1)} %slice.313), channel_id=1, source_target_pairs={{0,4},{4,8},{8,12},{12,16},{16,20},{20,24},{24,28},{1,5},{5,9},{9,... | collective-permute-start | bytes 299528 | tf_op jit(solution)/shard_map/ppermute | solution.py:17
  149.1 0.0 all-gather.3.cloned.1.call-update
  149.1 0.0 reduce-scatter.2.cloned.1.call-start
  149.2 0.0 copy-start.11
  149.2 0.0 copy-start.13
  149.2 2.6 %fusion.115 = (bf16[768,512]{1,0:T(8,128)(2,1)}, bf16[768,512]{1,0:T(8,128)(2,1)}) fusion(bf16[768,2304]{1,0:T(8,128)(2,1)} %shard_map.163), kind=kLoop, calls=%fused_computation.227 | loop fusion | bytes 3145728 | tf_op jit(solution)/shard_map/slice | solution.py:308
  151.8 0.6 slice_convert_fusion.29
  152.5 0.7 slice_convert_fusion.30
  153.2 0.1 broadcast_in_dim.2
  153.3 0.0 copy-start.44
  153.3 0.0 copy-start.8
  153.4 0.0 copy-start.12
  153.4 1.8 copy.20
  155.3 1.1 slice_bitcast_fusion.3
  156.4 0.6 convert_element_type.132
  157.0 0.6 convert_element_type.131
  157.6 0.2 maximum_convert_fusion
  157.8 0.9 fusion.8
  158.7 0.7 copy-done.4
  159.4 1.2 fusion.117
  160.6 2.0 convert_multiply_fusion.3.b_ref
  162.6 0.0 copy-start.2
  162.6 8.7 %shard_map.164 = (f32[768,640]{1,0:T(8,128)S(1)}, f32[768,640]{1,0:T(8,128)S(1)}) custom-call(f32[768,640]{1,0:T(8,128)S(1)} %get-tuple-element.79.a_ref, f32[768,640]{1,0:T(8,128)S(1)} %convert_multiply_fusion.3.b_ref), custom_call_target="tpu_custom_call" | custom-call | flops 1966080 | bytes 7864320 | tf_op jit(solution)/shard_map/pallas_call | solution.py:242
  171.4 6.8 %shard_map.165 = f32[8,8,640]{2,1,0:T(8,128)S(1)} custom-call(f32[8,640]{1,0:T(8,128)S(1)} %select_maximum_fusion.x_ref), custom_call_target="tpu_custom_call" | custom-call | bytes 10000000 | tf_op jit(solution)/shard_map/pallas_call | solution.py:196
  178.6 0.6 divide_multiply_fusion
  179.5 7.4 %fusion.113 = (f32[768]{0:T(1024)S(1)}, f32[768]{0:T(1024)S(1)}, f32[768,512]{1,0:T(8,128)}) fusion(f32[798,512]{1,0:T(8,128)S(1)} %divide_multiply_fusion, f32[512]{0:T(512)S(1)} %bitcast.72, f32[512]{0:T(512)S(1)} %bitcast.73, f32[512]{0:T(512)S(1)} %bitcast.75, f32[512]{0:T(512)S(1)} %bitcast.76, f32[512]{0:T(512)S(1)} %bitcast.77, f32[512]{0:T(512)S(1)} %bitcast.78, ...), kind=kLoop, calls=%fused_computation.226 | loop fusion | flops 25164288 | bytes 50401280 | tf_op jit(solution)/shard_map/reduce_sum | solution.py:327
  186.9 6.3 %all-reduce.9 = (f32[768]{0:T(1024)S(1)}, f32[768]{0:T(1024)S(1)}) all-reduce(f32[768]{0:T(1024)S(1)} %get-tuple-element.10, f32[768]{0:T(1024)S(1)} %get-tuple-element.9), channel_id=1, replica_groups=mesh['sp'=8,'tp'=4] {'tp'}, use_global_device_ids=true, to_apply=%region_4.0 | all-reduce | flops 1536 | bytes 12288 | tf_op jit(solution)/shard_map/psum | solution.py:326
  193.2 0.1 slice_reduce_fusion.8
  193.4 0.0 all-gather.5.cloned.1.call-done
  193.5 8.3 %fusion.54 = f32[768,2048]{1,0:T(8,128)} fusion(bf16[640,2048]{1,0:T(8,128)(2,1)} %all-gather.5.cloned.1.call-done, f32[768,640]{1,0:T(8,128)} %copy-done, f32[768,640]{1,0:T(8,128)S(1)} %get-tuple-element.8, bf16[768,2304]{1,0:T(8,128)(2,1)} %shard_map.163, f32[640]{0:T(1024)S(1)} %add_select_fusion), kind=kOutput, calls=%fused_computation.109 | convolution fusion | flops 2019655680 | bytes 13830656 | tf_op jit(solution)/shard_map/dot_general | solution.py:352
  201.8 7.2 %add_convert_fusion = bf16[768,2048]{1,0:T(8,128)(2,1)} fusion(f32[768,2048]{1,0:T(8,128)} %fusion.54, bf16[512,2048]{1,0:T(8,128)(2,1)} %all-gather.3.cloned.1.call-done, f32[768,512]{1,0:T(8,128)S(1)} %copy-done.5, f32[512]{0:T(512)S(1)} %copy-done.45, f32[512]{0:T(512)} %convert_element_type.131, f32[768]{0:T(1024)S(1)} %get-tuple-element.78, ...), kind=kOutput, calls=%fused_computation | convolution fusion | flops 1617297408 | bytes 13117440 | tf_op jit(solution)/shard_map/dot_general | solution.py:351
  209.0 0.0 reduce-scatter.2.cloned.1.call-update
  209.0 38.8 %reduce-scatter.2.cloned.1.call-done = bf16[192,2048]{1,0:T(8,128)(2,1)} async-done(((bf16[768,2048]{1,0:T(8,128)(2,1)}), bf16[192,2048]{1,0:T(8,128)(2,1)}) %reduce-scatter.2.cloned.1.call-update) | async-done | bytes 786448 | tf_op jit(solution)/shard_map/reduce_scatter | solution.py:349
  (99 shorter events, 0.3 us)
Async XLA Ops:
  6.5 2.8 %copy-start.1 = (bf16[192,2048]{1,0:T(8,128)(2,1)S(1)}, bf16[192,2048]{1,0:T(8,128)(2,1)}, u32[]{:S(2)}) copy-start(bf16[192,2048]{1,0:T(8,128)(2,1)} %param.17) | copy-start | bytes 2359300
  6.5 186.9 %all-gather.5.cloned.1.call-start = ((), (), s32[]{:S(2)}) async-start(), calls=%async_computation.2 | async-start | bytes 2949120 | tf_op jit(solution)/shard_map/all_gather | solution.py:312
  7.3 194.5 %all-gather.3.cloned.1.call-start = ((), (), s32[]{:S(2)}) async-start(), calls=%async_computation.1 | async-start | bytes 2359296 | tf_op jit(solution)/shard_map/all_gather | solution.py:311
  9.4 1.0 copy-start.6
  9.4 1.1 copy-start.7
  9.4 1.1 copy-start.9
  9.4 1.2 copy-start.10
  146.5 11.1 %collective-permute-start = (bf16[30,1664]{1,0:T(8,128)(2,1)S(1)}, bf16[30,1664]{1,0:T(8,128)(2,1)S(1)}, u32[]{:S(2)}, u32[]{:S(2)}) collective-permute-start(bf16[30,1664]{1,0:T(8,128)(2,1)S(1)} %slice.313), channel_id=1, source_target_pairs={{0,4},{4,8},{8,12},{12,16},{16,20},{20,24},{24,28},{1,5},{5,9},{9,... | collective-permute-start | bytes 299528 | tf_op jit(solution)/shard_map/ppermute | solution.py:17
  149.1 98.7 %reduce-scatter.2.cloned.1.call-start = ((), (), s32[]{:S(2)}) async-start(), calls=%async_computation.3 | async-start | bytes 3932160 | tf_op jit(solution)/shard_map/reduce_scatter | solution.py:349
  149.2 2.7 %copy-start.11 = (bf16[31,512]{1,0:T(8,128)(2,1)S(1)}, bf16[31,512]{1,0:T(8,128)(2,1)}, u32[]{:S(2)}) copy-start(bf16[31,512]{1,0:T(8,128)(2,1)} %param.23) | copy-start | bytes 95236
  149.2 4.0 %copy-start.13 = (f32[768,4]{0,1:T(4,128)S(1)}, f32[768,4]{0,1:T(4,128)}, u32[]{:S(2)}) copy-start(f32[768,4]{0,1:T(4,128)} %param.30) | copy-start | bytes 36868
  153.3 1.9 copy-start.44
  153.3 1.9 copy-start.8
  153.3 3.1 %copy-start.46 = (bf16[512]{0:T(512)(128)(2,1)S(1)}, bf16[512]{0:T(512)(128)(2,1)}, u32[]{:S(2)}) copy-start(bf16[512]{0:T(512)(128)(2,1)} %param.25) | copy-start | bytes 3076
  153.4 3.6 %copy-start.47 = (bf16[512]{0:T(512)(128)(2,1)S(1)}, bf16[512]{0:T(512)(128)(2,1)}, u32[]{:S(2)}) copy-start(bf16[512]{0:T(512)(128)(2,1)} %param.24) | copy-start | bytes 3076
  153.4 4.2 %copy-start.12 = (bf16[4,640]{1,0:T(4,128)(2,1)S(1)}, bf16[4,640]{1,0:T(4,128)(2,1)}, u32[]{:S(2)}) copy-start(bf16[4,640]{1,0:T(4,128)(2,1)} %param.26) | copy-start | bytes 15364
  155.2 2.4 slice-start
  157.8 1.5 copy-start.4
  162.6 15.7 %copy-start.2 = (bf16[768,512]{1,0:T(8,128)(2,1)S(1)}, bf16[768,512]{1,0:T(8,128)(2,1)}, u32[]{:S(2)}) copy-start(bf16[768,512]{1,0:T(8,128)(2,1)} %get-tuple-element.34) | copy-start | bytes 2359300
  162.6 15.7 %copy-start.3 = (bf16[768,512]{1,0:T(8,128)(2,1)S(1)}, bf16[768,512]{1,0:T(8,128)(2,1)}, u32[]{:S(2)}) copy-start(bf16[768,512]{1,0:T(8,128)(2,1)} %get-tuple-element.35) | copy-start | bytes 2359300
  171.3 7.8 %copy-start = (f32[768,640]{1,0:T(8,128)}, f32[768,640]{1,0:T(8,128)S(1)}, u32[]{:S(2)}) copy-start(f32[768,640]{1,0:T(8,128)S(1)} %get-tuple-element.7) | copy-start | bytes 5898244
  178.3 0.9 copy-start.14
  178.3 0.9 copy-start.15
  178.3 0.9 copy-start.16
  178.3 0.9 copy-start.17
  178.3 0.9 copy-start.18
  178.3 0.9 copy-start.19
  178.3 0.9 copy-start.20
  178.3 0.9 copy-start.21
  178.4 0.9 copy-start.22
  178.4 0.9 copy-start.23
  178.4 0.9 copy-start.24
  178.4 0.9 copy-start.25
  178.4 0.9 copy-start.26
  178.4 0.9 copy-start.27
  178.4 0.9 copy-start.28
  178.4 0.9 copy-start.29
  178.4 0.9 copy-start.30
  178.4 0.9 copy-start.31
  178.5 0.9 copy-start.32
  178.5 0.9 copy-start.33
  178.5 0.9 copy-start.34
  178.5 0.9 copy-start.35
  178.5 0.9 copy-start.36
  178.5 0.9 copy-start.37
  179.5 13.9 %copy-start.43 = (f32[640]{0:T(1024)S(1)}, f32[640]{0:T(1024)}, u32[]{:S(2)}) copy-start(f32[640]{0:T(1024)} %param.31) | copy-start | bytes 7684
  193.4 8.4 %copy-start.5 = (f32[768,512]{1,0:T(8,128)S(1)}, f32[768,512]{1,0:T(8,128)}, u32[]{:S(2)}) copy-start(f32[768,512]{1,0:T(8,128)} %get-tuple-element.33) | copy-start | bytes 4718596
  193.4 8.4 %copy-start.45 = (f32[512]{0:T(512)S(1)}, f32[512]{0:T(512)}, u32[]{:S(2)}) copy-start(f32[512]{0:T(512)} %convert_element_type.132) | copy-start | bytes 6148
  (5 other events, 4.5 us)
Sparse Core Ops, SparseCore 0:
  9.4 87.0 all-gather.4
  149.3 48.6 all-gather.2
  209.2 38.6 reduce-scatter.1
